TPU v7x, 256 devices: a 4x2x16 block of a 4x16x16 slice. The times are simulated.
256 devices in a mesh: grp: 2 (over y), fs: 32 (over z, core), tp: 4 (over x).
Axes of the slice: x: 4, y: 2, z: 16, core: 2. Of those that a mesh axis runs over, the one named last changes fastest.
The devices are a block of a 4x16x16 slice.
Arguments:
- tokens: bfloat16 [1536, 2048], P(('grp', 'tp')), parts along dimension 0, may hold values from -6 to 6
- norm_gain: float32 [2048], P('fs'), may hold values from 0.1 to 1.9
- up_trained: float32 [2048, 8192], P('fs', 'tp'), may hold values from -0.125 to 0.125
- down_trained: float32 [2048, 8192], P('fs', 'tp'), may hold values from -0.125 to 0.125
Outputs:
- up_serving: bfloat16 [4096, 8192], P('grp', 'fs'), parts along dimension 0
- down_serving: bfloat16 [4096, 8192], P('grp', 'fs'), parts along dimension 0
- prompt_output: bfloat16 [1536, 2048], P(('grp', 'tp'), 'fs'), parts along dimension 0
There are 2 independent parts, one for each index of `grp`. A program takes and returns all parts, laid end to end along the dimension named above; an argument that names none is the same for every part. Nothing has to cross between parts.
All inputs are finite; a program needn't handle non-finite values.
Results may differ from a plain program's by a relative error of at most 0.0074.
Values may be sent and summed in bfloat16 or wider, within the bound.
No kernel may reach another device: no remote copies, remote signals or barrier semaphores. Data moves between devices by JAX's collectives and lax.ppermute only.
A program may use at most 64 MiB of HBM per device.

v0:
```python
import jax
import jax.numpy as jnp
from jax import lax
from jax.sharding import PartitionSpec as P

epsilon = 1e-06


def joined_along(parts, dim):
    parts = jnp.moveaxis(parts, 0, dim)
    dims = parts.shape
    return parts.reshape(*dims[:dim], dims[dim] * dims[dim + 1], *dims[dim + 2 :])


def copy_for_each(x, axis):
    devices = lax.axis_size(axis)
    return lax.all_to_all(jnp.broadcast_to(x[None], (devices, *x.shape)), axis, 0, 0, tiled=True)


def collect(x, axis, dim):
    return joined_along(copy_for_each(x, axis), dim)


def in_blocks(x, dim, devices):
    dims = x.shape
    parts = x.reshape(*dims[:dim], devices, dims[dim] // devices, *dims[dim + 1 :])
    return jnp.moveaxis(parts, dim, 0)


def sum_at_owner(x, axis, dim):
    parts = in_blocks(x, dim, lax.axis_size(axis))
    arrived = lax.all_to_all(parts, axis, split_axis=0, concat_axis=0, tiled=True)
    return arrived.astype(jnp.float32).sum(axis=0)


def local(tokens, norm_gain, up_trained, down_trained):
    shards = lax.axis_size("fs")
    groups = lax.axis_size("tp")
    rows_local = up_trained.shape[0]
    cols_local = up_trained.shape[1]
    folded = (norm_gain[:, None] * up_trained).astype(jnp.bfloat16)
    stacked = jnp.stack([folded, down_trained.astype(jnp.bfloat16)])
    served_width = cols_local * groups // shards
    blocks_here = cols_local // served_width
    quarter_rows = rows_local // groups
    pieces = stacked.reshape(2, groups, quarter_rows, blocks_here, served_width)
    moved = lax.all_to_all(pieces, "tp", split_axis=1, concat_axis=3, tiled=True)
    placed = lax.all_to_all(moved, "fs", split_axis=3, concat_axis=2, tiled=True)
    ordered = placed.reshape(2, shards, quarter_rows, served_width)
    joined = collect(ordered, "tp", 2)
    owned = joined.reshape(2, rows_local * shards, served_width)
    up_serving = owned[0]
    down_serving = owned[1]
    values = tokens.astype(jnp.float32)
    scale = lax.rsqrt(jnp.mean(values * values, axis=1, keepdims=True) + epsilon)
    normed = (values * scale).astype(jnp.bfloat16)
    hidden = jnp.dot(normed, up_serving, preferred_element_type=jnp.float32)
    active = jnp.square(jax.nn.relu(hidden)).astype(jnp.bfloat16)
    summed = sum_at_owner(
        lax.dot_general(
            down_serving, active, (((1,), (1,)), ((), ())), preferred_element_type=jnp.float32
        ).astype(jnp.bfloat16),
        "fs",
        0,
    )
    prompt_output = summed.T.astype(jnp.bfloat16)
    return (up_serving, down_serving, prompt_output)


def solution(mesh):
    in_specs = (P(("grp", "tp"), None), P("fs"), P("fs", "tp"), P("fs", "tp"))
    out_specs = (P("grp", "fs"), P("grp", "fs"), P(("grp", "tp"), "fs"))
    return jax.shard_map(local, mesh=mesh, in_specs=in_specs, out_specs=out_specs, check_vma=False)
```

profile of v0, /device:TPU:33, one launch (start us, length us, event | category | flops | bytes accessed | tf_op | source)
XLA Modules:
  0.0 171.2 jit_solution(14890770866300171647)
XLA Ops:
  0.6 0.0 copy-start.3
  0.6 1.2 multiply_convert_fusion
  1.8 0.1 copy.23
  1.9 0.0 copy-done.3
  2.0 0.1 copy.24
  2.0 0.1 pad_maximum_fusion
  2.1 11.9 %all_to_all.43 = bf16[2,4,16,8,256]{4,3,2,0,1:T(8,128)(2,1)S(1)} all-to-all(bf16[2,4,16,8,256]{4,3,2,0,1:T(8,128)(2,1)S(1)} %copy.17), channel_id=1, replica_groups=mesh['grp'=2,'fs'=32,'tp'=4] {'tp'}, dimensions={1} | all-to-all | bytes 1048576 | tf_op jit(solution)/shard_map/all_to_all | solution.py:47
  14.0 0.1 copy.28
  14.0 0.3 copy.19
  14.3 60.6 %all_to_all.44 = bf16[2,1,16,32,256]{4,2,0,1,3:T(8,128)(2,1)S(1)} all-to-all(bf16[2,1,16,32,256]{4,2,0,1,3:T(8,128)(2,1)S(1)} %copy.19), channel_id=1, replica_groups=mesh['grp'=2,'fs'=32,'tp'=4] {'fs'}, dimensions={3} | all-to-all | bytes 1048576 | tf_op jit(solution)/shard_map/all_to_all | solution.py:48
  75.0 1.5 broadcast_in_dim.10
  76.5 0.0 copy-start.2
  76.5 3.8 %all-to-all-start.2 = ((bf16[4,2,32,16,256]{4,3,2,1,0:T(8,128)(2,1)}), bf16[4,2,32,16,256]{4,3,2,1,0:T(8,128)(2,1)S(1)}, u32[]{:S(2)}, u32[]{:S(2)}) async-start(bf16[4,2,32,16,256]{4,3,2,1,0:T(8,128)(2,1)} %broadcast_in_dim.10), calls=%async_computation.2 | async-start | bytes 4194304 | tf_op jit(solution)/shard_map/all_to_all | solution.py:17
  80.4 0.0 copy-done.2
  80.4 0.2 fusion
  80.6 25.6 %all-to-all-done.2 = bf16[4,2,32,16,256]{4,3,2,1,0:T(8,128)(2,1)S(1)} async-done(((bf16[4,2,32,16,256]{4,3,2,1,0:T(8,128)(2,1)}), bf16[4,2,32,16,256]{4,3,2,1,0:T(8,128)(2,1)S(1)}, u32[]{:S(2)}, u32[]{:S(2)}) %all-to-all-start.2) | async-done | bytes 2097184 | tf_op jit(solution)/shard_map/all_to_all | solution.py:17
  106.2 0.3 copy.27
  106.5 0.2 fusion.10
  106.8 0.0 copy-start.1
  106.8 0.0 copy-start
  106.8 0.9 copy-done.1
  107.7 2.3 %convolution_convert_fusion = bf16[2048,192]{0,1:T(8,128)(2,1)S(1)} fusion(bf16[2048,256]{1,0:T(8,128)(2,1)S(1)} %bitcast.29, bf16[2048,256]{1,0:T(8,128)(2,1)S(1)} %bitcast.31, bf16[192,2048]{1,0:T(8,128)(2,1)} %param.4, f32[192]{0:T(256)S(1)} %add_rsqrt_fusion), kind=kOutput, calls=%fused_computation | convolution fusion | flops 404373504 | bytes 3670784 | tf_op jit(solution)/shard_map/dot_general | solution.py:60
  110.0 0.0 copy-done
  110.0 0.5 copy.22
  110.5 59.9 %all_to_all.45 = bf16[32,64,192]{2,1,0:T(8,128)(2,1)S(1)} all-to-all(bf16[32,64,192]{2,1,0:T(8,128)(2,1)S(1)} %bitcast.28), channel_id=1, replica_groups=mesh['grp'=2,'fs'=32,'tp'=4] {'fs'}, dimensions={0} | all-to-all | bytes 1572864 | tf_op jit(solution)/shard_map/all_to_all | solution.py:32
  170.4 0.8 reduce_sum.22
  (4 shorter events, 0.1 us)
Async XLA Ops:
  0.6 1.3 copy-start.3
  76.5 3.8 %copy-start.2 = (bf16[192,2048]{1,0:T(8,128)(2,1)S(1)}, bf16[192,2048]{1,0:T(8,128)(2,1)}, u32[]{:S(2)}) copy-start(bf16[192,2048]{1,0:T(8,128)(2,1)} %param.4) | copy-start | bytes 2359300
  76.5 29.7 %all-to-all-start.2 = ((bf16[4,2,32,16,256]{4,3,2,1,0:T(8,128)(2,1)}), bf16[4,2,32,16,256]{4,3,2,1,0:T(8,128)(2,1)S(1)}, u32[]{:S(2)}, u32[]{:S(2)}) async-start(bf16[4,2,32,16,256]{4,3,2,1,0:T(8,128)(2,1)} %broadcast_in_dim.10), calls=%async_computation.2 | async-start | bytes 4194304 | tf_op jit(solution)/shard_map/all_to_all | solution.py:17
  106.8 1.0 copy-start.1
  106.8 3.3 %copy-start = (bf16[1,32,4,16,256]{4,3,2,1,0:T(8,128)(2,1)}, bf16[1,32,4,16,256]{4,3,2,1,0:T(8,128)(2,1)S(1)}, u32[]{:S(2)}) copy-start(bf16[1,32,4,16,256]{4,3,2,1,0:T(8,128)(2,1)S(1)} %get-tuple-element.3) | copy-start | bytes 3145732
where the time goes:
time: 172 us; the launch traced here: 171 us
  blocking collectives  132 us (77%)
  waiting for transfers between devices  25.6 us (15%)
  local copies, waits for them, and re-layouts  4.06 us (2%)
  starting transfers between devices  3.83 us (2%)
  other arithmetic  2.33 us (1%)
  matrix products  2.28 us (1%)
    all_to_all x1, blocking collectives, local(): lax.all_to_all(moved, 'fs', split_axis=3, concat_axis=2, tiled=True)  60.6 us
    all_to_all x1, blocking collectives, sum_at_owner(): lax.all_to_all(parts, axis, split_axis=0, concat_axis=0, tiled=True)  59.9 us
    all_to_all x1, waiting for transfers between devices, copy_for_each(): lax.all_to_all(jnp.broadcast_to(x[None], (devices, *x.shape)), axis, 0, 0...  25.6 us
    all_to_all x1, blocking collectives, local(): lax.all_to_all(pieces, 'tp', split_axis=1, concat_axis=3, tiled=True)  11.9 us
    all_to_all x1, starting transfers between devices, copy_for_each(): lax.all_to_all(jnp.broadcast_to(x[None], (devices, *x.shape)), axis, 0, 0...  3.83 us
  transfers between devices with their start and end apart: 1, of which 1 were waited for; matrix products, arithmetic and copies ran while one was open for 0% of the time, Pallas kernels for 0%

commit v1 on v0

--- a/solution.py
+++ b/solution.py
@@ -44,7 +44,10 @@
     blocks_here = cols_local // served_width
     quarter_rows = rows_local // groups
     pieces = stacked.reshape(2, groups, quarter_rows, blocks_here, served_width)
-    moved = lax.all_to_all(pieces, "tp", split_axis=1, concat_axis=3, tiled=True)
+    moved = jnp.concatenate(
+        lax.all_to_all(jnp.stack(jnp.split(pieces, lax.axis_size("tp"), axis=1)), "tp", 0, 0),
+        axis=3,
+    )
     placed = lax.all_to_all(moved, "fs", split_axis=3, concat_axis=2, tiled=True)
     ordered = placed.reshape(2, shards, quarter_rows, served_width)
     joined = collect(ordered, "tp", 2)

time: 172 us -> 172 us (level)
  no operation moved by 1% of the time
where the time goes in v1:
time: 172 us; the launch traced here: 171 us
  blocking collectives  132 us (77%)
  waiting for transfers between devices  25.6 us (15%)
  local copies, waits for them, and re-layouts  4.1 us (2%)
  starting transfers between devices  3.83 us (2%)
  other arithmetic  2.35 us (1%)
  matrix products  2.28 us (1%)
    all_to_all x1, blocking collectives, local(): lax.all_to_all(moved, 'fs', split_axis=3, concat_axis=2, tiled=True)  60.6 us
    all_to_all x1, blocking collectives, sum_at_owner(): lax.all_to_all(parts, axis, split_axis=0, concat_axis=0, tiled=True)  59.9 us
    all_to_all x1, waiting for transfers between devices, copy_for_each(): lax.all_to_all(jnp.broadcast_to(x[None], (devices, *x.shape)), axis, 0, 0...  25.6 us
    all_to_all x1, blocking collectives, local(): lax.all_to_all(jnp.stack(jnp.split(pieces, lax.axis_size('tp'), axis=1)),...  11.9 us
    all_to_all x1, starting transfers between devices, copy_for_each(): lax.all_to_all(jnp.broadcast_to(x[None], (devices, *x.shape)), axis, 0, 0...  3.83 us
  transfers between devices with their start and end apart: 1, of which 1 were waited for; matrix products, arithmetic and copies ran while one was open for 0% of the time, Pallas kernels for 0%

profile of v1, /device:TPU:33, one launch (start us, length us, event | category | flops | bytes accessed | tf_op | source)
XLA Modules:
  0.0 171.3 jit_solution(8238245732470622239)
XLA Ops:
  0.6 0.0 copy-start.3
  0.6 1.2 multiply_convert_fusion
  1.8 0.1 copy.24
  1.9 0.0 copy-done.3
  2.0 0.1 copy.25
  2.1 0.1 pad_maximum_fusion
  2.2 11.9 %all_to_all.30 = bf16[4,2,1,16,8,256]{5,4,3,1,2,0:T(8,128)(2,1)S(1)} all-to-all(bf16[4,2,1,16,8,256]{5,4,3,1,2,0:T(8,128)(2,1)S(1)} %pad_maximum_fusion), channel_id=1, replica_groups=mesh['grp'=2,'fs'=32,'tp'=4] {'tp'}, dimensions={0} | all-to-all | bytes 1048576 | tf_op jit(solution)/shard_map/all_to_all | solution.py:48
  14.0 0.1 copy.29
  14.1 0.3 copy.20
  14.4 60.6 %all_to_all.31 = bf16[2,1,16,32,256]{4,2,0,1,3:T(8,128)(2,1)S(1)} all-to-all(bf16[2,1,16,32,256]{4,2,0,1,3:T(8,128)(2,1)S(1)} %copy.20), channel_id=1, replica_groups=mesh['grp'=2,'fs'=32,'tp'=4] {'fs'}, dimensions={3} | all-to-all | bytes 1048576 | tf_op jit(solution)/shard_map/all_to_all | solution.py:51
  75.1 1.5 broadcast_in_dim.10
  76.6 0.0 copy-start.2
  76.6 3.8 %all-to-all-start.2 = ((bf16[4,2,32,16,256]{4,3,2,1,0:T(8,128)(2,1)}), bf16[4,2,32,16,256]{4,3,2,1,0:T(8,128)(2,1)S(1)}, u32[]{:S(2)}, u32[]{:S(2)}) async-start(bf16[4,2,32,16,256]{4,3,2,1,0:T(8,128)(2,1)} %broadcast_in_dim.10), calls=%async_computation.2 | async-start | bytes 4194304 | tf_op jit(solution)/shard_map/all_to_all | solution.py:17
  80.4 0.0 copy-done.2
  80.4 0.2 fusion
  80.7 25.6 %all-to-all-done.2 = bf16[4,2,32,16,256]{4,3,2,1,0:T(8,128)(2,1)S(1)} async-done(((bf16[4,2,32,16,256]{4,3,2,1,0:T(8,128)(2,1)}), bf16[4,2,32,16,256]{4,3,2,1,0:T(8,128)(2,1)S(1)}, u32[]{:S(2)}, u32[]{:S(2)}) %all-to-all-start.2) | async-done | bytes 2097184 | tf_op jit(solution)/shard_map/all_to_all | solution.py:17
  106.3 0.3 copy.28
  106.6 0.2 fusion.10
  106.8 0.0 copy-start.1
  106.8 0.0 copy-start
  106.8 0.9 copy-done.1
  107.8 2.3 %convolution_convert_fusion = bf16[2048,192]{0,1:T(8,128)(2,1)S(1)} fusion(bf16[2048,256]{1,0:T(8,128)(2,1)S(1)} %bitcast.37, bf16[2048,256]{1,0:T(8,128)(2,1)S(1)} %bitcast.39, bf16[192,2048]{1,0:T(8,128)(2,1)} %param.4, f32[192]{0:T(256)S(1)} %add_rsqrt_fusion), kind=kOutput, calls=%fused_computation | convolution fusion | flops 404373504 | bytes 3670784 | tf_op jit(solution)/shard_map/dot_general | solution.py:63
  110.1 0.0 copy-done
  110.1 0.5 copy.23
  110.6 59.9 %all_to_all.32 = bf16[32,64,192]{2,1,0:T(8,128)(2,1)S(1)} all-to-all(bf16[32,64,192]{2,1,0:T(8,128)(2,1)S(1)} %bitcast.36), channel_id=1, replica_groups=mesh['grp'=2,'fs'=32,'tp'=4] {'fs'}, dimensions={0} | all-to-all | bytes 1572864 | tf_op jit(solution)/shard_map/all_to_all | solution.py:32
  170.5 0.8 reduce_sum.22
  (6 shorter events, 0.1 us)
Async XLA Ops:
  0.6 1.3 copy-start.3
  76.6 3.8 %copy-start.2 = (bf16[192,2048]{1,0:T(8,128)(2,1)S(1)}, bf16[192,2048]{1,0:T(8,128)(2,1)}, u32[]{:S(2)}) copy-start(bf16[192,2048]{1,0:T(8,128)(2,1)} %param.4) | copy-start | bytes 2359300
  76.6 29.7 %all-to-all-start.2 = ((bf16[4,2,32,16,256]{4,3,2,1,0:T(8,128)(2,1)}), bf16[4,2,32,16,256]{4,3,2,1,0:T(8,128)(2,1)S(1)}, u32[]{:S(2)}, u32[]{:S(2)}) async-start(bf16[4,2,32,16,256]{4,3,2,1,0:T(8,128)(2,1)} %broadcast_in_dim.10), calls=%async_computation.2 | async-start | bytes 4194304 | tf_op jit(solution)/shard_map/all_to_all | solution.py:17
  106.8 1.0 copy-start.1
  106.8 3.3 %copy-start = (bf16[1,32,4,16,256]{4,3,2,1,0:T(8,128)(2,1)}, bf16[1,32,4,16,256]{4,3,2,1,0:T(8,128)(2,1)S(1)}, u32[]{:S(2)}) copy-start(bf16[1,32,4,16,256]{4,3,2,1,0:T(8,128)(2,1)S(1)} %get-tuple-element.3) | copy-start | bytes 3145732
